TPU v7x, 32 devices: a whole 2x2x4 slice. The times are simulated.
32 devices in a mesh: grp: 2 (over x), ep: 16 (over z, y, core).
Axes of the slice: x: 2, y: 2, z: 4, core: 2. Of those that a mesh axis runs over, the one named last changes fastest.
Arguments:
- tokens: bfloat16 [1024, 2048], P(('grp', 'ep')), parts along dimension 0, may hold values from -6 to 6
- norm_gain: float32 [2048], replicated, may hold values from 0.1 to 1.9
- routing: int32 [1024, 8], P(('grp', 'ep')), parts along dimension 0, may hold values from 0 to 15, all different within a row; in each aligned block of 32 rows (0 to 31, 32 to 63, ...) at most 32 rows name the same one
- gates: float32 [1024, 8], P(('grp', 'ep')), parts along dimension 0, may hold values from 0.05 to 0.6
- w_gate: bfloat16 [16, 2048, 512], P('ep'), may hold values from -0.125 to 0.125
- w_up: bfloat16 [16, 2048, 512], P('ep'), may hold values from -0.125 to 0.125
- w_down: bfloat16 [16, 512, 2048], P('ep'), may hold values from -0.25 to 0.25
- shared_gate: bfloat16 [2048, 512], replicated, may hold values from -0.125 to 0.125
- shared_up: bfloat16 [2048, 512], replicated, may hold values from -0.125 to 0.125
- shared_down: bfloat16 [512, 2048], replicated, may hold values from -0.25 to 0.25
Outputs:
- mixed: bfloat16 [1024, 2048], P(('grp', 'ep')), parts along dimension 0
There are 2 independent parts, one for each index of `grp`. A program takes and returns all parts, laid end to end along the dimension named above; an argument that names none is the same for every part. Nothing has to cross between parts.
Inputs may be any that keep to these rules, and one draw needn't show every extreme that they name: `routing`: within the 32 rows of one device no expert is named by more than 32 rows, and in every draw some expert is named by exactly 32 rows of some device; each row names 8 different experts.
All inputs are finite; a program needn't handle non-finite values.
Results may differ from a plain program's by a relative error of at most 0.0067.
Values may be sent and summed in bfloat16 or wider, within the bound.
A program may use at most 128 MiB of HBM per device.

v0:
```python
import jax
import jax.numpy as jnp
from jax import lax
from jax.sharding import PartitionSpec as P

epsilon = 1e-06


def rms_normed(tokens, norm_gain):
    floats = tokens.astype(jnp.float32)
    scale_inv = lax.rsqrt(jnp.mean(floats * floats, axis=-1, keepdims=True) + epsilon)
    return (floats * scale_inv * norm_gain).astype(jnp.bfloat16)


def expert_outputs(buffer, w_gate, w_up, w_down):
    gate_act = jnp.einsum("nesd,edf->nesf", buffer, w_gate, preferred_element_type=jnp.float32)
    up_act = jnp.einsum("nesd,edf->nesf", buffer, w_up, preferred_element_type=jnp.float32)
    hidden = (jax.nn.silu(gate_act) * up_act).astype(jnp.bfloat16)
    return jnp.einsum("nesf,efd->nesd", hidden, w_down, preferred_element_type=jnp.float32).astype(
        jnp.bfloat16
    )


def slot_targets(routing, expert_count, slot_count):
    leading = routing.shape[:-2]
    tok_count, top_count = routing.shape[-2:]
    flattened = routing.reshape(leading + (tok_count * top_count,))
    onehot = (flattened[..., None] == jnp.arange(expert_count, dtype=jnp.int32)).astype(jnp.int32)
    earlier = jnp.cumsum(onehot, axis=-2) - onehot
    within = jnp.sum(earlier * onehot, axis=-1)
    return (flattened * slot_count + within).reshape(routing.shape)


def slot_tables(targets, gates, row_count):
    slot_ids = jnp.arange(row_count, dtype=jnp.int32)
    matches = targets[..., None] == slot_ids
    selected = jnp.any(matches, axis=-2)
    weights = jnp.sum(
        jnp.where(matches, gates[..., None], jnp.zeros_like(gates[..., None])), axis=-2
    )
    return (selected, weights)


def body(
    tokens, norm_gain, routing, gates, w_gate, w_up, w_down, shared_gate, shared_up, shared_down
):
    normed = rms_normed(tokens, norm_gain)
    shared_hidden = (
        jax.nn.silu(jnp.dot(normed, shared_gate, preferred_element_type=jnp.float32))
        * jnp.dot(normed, shared_up, preferred_element_type=jnp.float32)
    ).astype(jnp.bfloat16)
    shared_out = jnp.dot(shared_hidden, shared_down, preferred_element_type=jnp.float32)
    tok_count, top_count = routing.shape
    local_count = w_gate.shape[0]
    ep_size = lax.axis_size("ep")
    expert_count = local_count * ep_size
    slot_count = max(4, (2 * tok_count * top_count + expert_count - 1) // expert_count)
    model_width = normed.shape[1]
    targets = slot_targets(routing, expert_count, slot_count)
    selected, weights = slot_tables(targets, gates, expert_count * slot_count)
    buffer = jnp.einsum(
        "tr,td->rd", selected.astype(jnp.bfloat16), normed, preferred_element_type=jnp.float32
    ).astype(jnp.bfloat16)
    buffer = buffer.reshape(ep_size, local_count, slot_count, model_width)
    returned = lax.all_to_all(
        expert_outputs(
            lax.all_to_all(buffer, "ep", split_axis=0, concat_axis=0, tiled=True),
            w_gate,
            w_up,
            w_down,
        ),
        "ep",
        split_axis=0,
        concat_axis=0,
        tiled=True,
    )
    returned = returned.reshape(expert_count * slot_count, model_width)
    chosen_rows = returned[targets.reshape(-1)].reshape(tok_count, top_count, model_width)
    routed = jnp.sum(gates[..., None] * chosen_rows.astype(jnp.float32), axis=1)
    return (shared_out + routed).astype(jnp.bfloat16)


def solution(mesh):
    placed = (
        P(("grp", "ep"), None),
        P(),
        P(("grp", "ep"), None),
        P(("grp", "ep"), None),
        P("ep", None, None),
        P("ep", None, None),
        P("ep", None, None),
        P(),
        P(),
        P(),
    )
    return jax.shard_map(
        body, mesh=mesh, in_specs=placed, out_specs=P(("grp", "ep"), None), check_vma=False
    )
```

profile of v0, /device:TPU:15, one launch (start us, length us, event | category | flops | bytes accessed | tf_op | source)
XLA Modules:
  0.0 129.9 jit_solution(7531492811068998764)
XLA Ops:
  0.0 0.0 copy-start
  0.0 0.9 copy.26
  0.9 0.1 eq.42
  1.0 0.1 eq.38
  1.1 0.6 reduce-window.6
  1.7 0.2 slice_reduce_fusion
  1.9 0.1 fusion.53
  2.0 0.1 reduce_sum.33
  2.1 0.2 fusion.41
  2.4 1.0 fusion.42
  3.4 1.7 %convolution_convert_fusion.1 = bf16[512,2048]{1,0:T(8,128)(2,1)S(1)} fusion(pred[32,512]{1,0:T(8,128)(4,1)S(1)} %fusion.41, bf16[32,2048]{1,0:T(8,128)(2,1)} %param.10, f32[2048]{0:T(1024)} %param.11, f32[32]{0:T(128)S(1)} %add_rsqrt_fusion), kind=kOutput, calls=%fused_computation.2 | convolution fusion | flops 68419584 | bytes 2252928 | tf_op jit(solution)/shard_map/tr,td->rd/dot_general | solution.py:61
  5.1 0.0 copy-start.5
  5.1 53.7 %all_to_all.10 = bf16[16,1,32,2048]{3,2,1,0:T(8,128)(2,1)S(1)} all-to-all(bf16[16,1,32,2048]{3,2,1,0:T(8,128)(2,1)S(1)} %bitcast.105), channel_id=1, replica_groups=mesh['grp'=2,'ep'=16] {'ep'}, dimensions={0} | all-to-all | bytes 4194304 | tf_op jit(solution)/shard_map/all_to_all | solution.py:67
  58.8 0.0 copy-start.2
  58.8 1.3 copy-done.2
  60.1 0.0 copy-done.5
  60.1 1.2 fusion.10
  61.4 0.0 copy-done
  61.4 6.1 %fusion = bf16[16,1,32,2048]{3,2,1,0:T(8,128)(2,1)} fusion(bf16[1,512,2048]{2,1,0:T(8,128)(2,1)S(1)} %copy-done, bf16[1,2048,512]{2,1,0:T(8,128)(2,1)} %param.15, bf16[16,1,32,2048]{3,2,1,0:T(8,128)(2,1)} %copy-done.2, f32[16,1,32,512]{3,2,0,1:T(8,128)S(1)} %fusion.10), kind=kOutput, calls=%fused_computation.3 | convolution fusion | flops 2150105088 | bytes 9437184 | tf_op jit(solution)/shard_map/nesf,efd->nesd/dot_general | solution.py:19
  67.5 0.0 copy-start.4
  67.5 0.0 copy-start.1
  67.5 5.2 %all-to-all-start.1 = ((bf16[16,1,32,2048]{3,2,1,0:T(8,128)(2,1)}), bf16[16,1,32,2048]{3,2,1,0:T(8,128)(2,1)}, u32[]{:S(2)}, u32[]{:S(2)}) async-start(bf16[16,1,32,2048]{3,2,1,0:T(8,128)(2,1)} %fusion), calls=%async_computation.1 | async-start | bytes 4194304 | tf_op jit(solution)/shard_map/all_to_all | solution.py:65
  72.6 0.1 mul.75
  72.7 0.0 copy-done.4
  72.7 0.7 copy.25
  73.4 0.0 copy-done.1
  73.4 0.0 copy-done.3
  73.4 2.7 %fusion.61 = f32[32,512]{1,0:T(8,128)} fusion(bf16[2048,512]{1,0:T(8,128)(2,1)} %param.17, bf16[32,2048]{1,0:T(8,128)(2,1)S(1)} %copy-done.1, f32[2048]{0:T(1024)S(1)} %copy-done.3, f32[32]{0:T(128)S(1)} %add_rsqrt_fusion), kind=kOutput, calls=%fused_computation.52 | convolution fusion | flops 67371008 | bytes 2302080 | tf_op jit(solution)/shard_map/dot_general | solution.py:49
  76.2 44.0 %all-to-all-done.1 = bf16[16,1,32,2048]{3,2,1,0:T(8,128)(2,1)} async-done(((bf16[16,1,32,2048]{3,2,1,0:T(8,128)(2,1)}), bf16[16,1,32,2048]{3,2,1,0:T(8,128)(2,1)}, u32[]{:S(2)}, u32[]{:S(2)}) %all-to-all-start.1) | async-done | bytes 2097184 | tf_op jit(solution)/shard_map/all_to_all | solution.py:65
  120.1 4.2 %gather_fusion = bf16[256,2048]{1,0:T(8,128)(2,1)S(1)} fusion(bf16[512,2048]{1,0:T(8,128)(2,1)} %bitcast.23, s32[1024]{0:T(1024)S(1)} %pad_clamp_fusion), kind=kCustom, calls=%fused_computation | custom fusion | bytes 2098176 | tf_op jit(solution)/shard_map/gather | solution.py:78
  124.4 1.7 %fusion.2 = f32[32,2048]{1,0:T(8,128)S(1)} fusion(bf16[256,2048]{1,0:T(8,128)(2,1)S(1)} %gather_fusion, f32[32,8]{1,0:T(8,128)} %copy.25), kind=kLoop, calls=%fused_computation.7 | loop fusion | flops 1507328 | bytes 1311744 | tf_op jit(solution)/shard_map/reduce_sum | solution.py:79
  126.1 3.9 %fusion.1 = bf16[32,2048]{1,0:T(8,128)(2,1)} fusion(f32[32,2048]{1,0:T(8,128)S(1)} %fusion.2, bf16[512,2048]{1,0:T(8,128)(2,1)} %param.19, bf16[2048,512]{1,0:T(8,128)(2,1)} %param.18, f32[32,512]{1,0:T(8,128)} %fusion.61, bf16[32,2048]{1,0:T(8,128)(2,1)S(1)} %copy-done.1, f32[2048]{0:T(1024)S(1)} %copy-done.3, f32[32]{0:T(128)S(1)} %add_rsqrt_fusion), kind=kOutput, calls=%fused_computation.5 | convolution fusion | flops 134709248 | bytes 4792448 | tf_op jit(solution)/shard_map/dot_general | solution.py:52
  (8 shorter events, 0.1 us)
Async XLA Ops:
  0.0 61.4 %copy-start = (bf16[1,512,2048]{2,1,0:T(8,128)(2,1)S(1)}, bf16[1,512,2048]{2,1,0:T(8,128)(2,1)}, u32[]{:S(2)}) copy-start(bf16[1,512,2048]{2,1,0:T(8,128)(2,1)} %param.16) | copy-start | bytes 6291460
  5.1 55.0 %copy-start.5 = (bf16[1,2048,512]{2,1,0:T(8,128)(2,1)S(1)}, bf16[1,2048,512]{2,1,0:T(8,128)(2,1)}, u32[]{:S(2)}) copy-start(bf16[1,2048,512]{2,1,0:T(8,128)(2,1)} %param.14) | copy-start | bytes 6291460
  58.8 1.3 copy-start.2
  67.5 5.3 %copy-start.4 = (f32[32,8]{0,1:T(8,128)S(1)}, f32[32,8]{0,1:T(8,128)}, u32[]{:S(2)}) copy-start(f32[32,8]{0,1:T(8,128)} %param.13) | copy-start | bytes 3076
  67.5 6.0 %copy-start.1 = (bf16[32,2048]{1,0:T(8,128)(2,1)S(1)}, bf16[32,2048]{1,0:T(8,128)(2,1)}, u32[]{:S(2)}) copy-start(bf16[32,2048]{1,0:T(8,128)(2,1)} %param.10) | copy-start | bytes 393220
  67.5 6.0 %copy-start.3 = (f32[2048]{0:T(1024)S(1)}, f32[2048]{0:T(1024)}, u32[]{:S(2)}) copy-start(f32[2048]{0:T(1024)} %param.11) | copy-start | bytes 24580
  67.5 52.7 %all-to-all-start.1 = ((bf16[16,1,32,2048]{3,2,1,0:T(8,128)(2,1)}), bf16[16,1,32,2048]{3,2,1,0:T(8,128)(2,1)}, u32[]{:S(2)}, u32[]{:S(2)}) async-start(bf16[16,1,32,2048]{3,2,1,0:T(8,128)(2,1)} %fusion), calls=%async_computation.1 | async-start | bytes 4194304 | tf_op jit(solution)/shard_map/all_to_all | solution.py:65
where the time goes:
time: 130 us
  blocking collectives  53.7 us (41%)
  waiting for transfers between devices  44 us (34%)
  matrix products  15.6 us (12%)
  local copies, waits for them, and re-layouts  7.66 us (6%)
  starting transfers between devices  5.17 us (4%)
  other arithmetic  3.72 us (3%)
    all_to_all x1, blocking collectives, body(): lax.all_to_all(buffer, 'ep', split_axis=0, concat_axis=0, tiled=True)  53.7 us
    all_to_all x1, waiting for transfers between devices, body(): lax.all_to_all(expert_outputs(lax.all_to_all(buffer, 'ep', split_axis=0,...  44 us
    dot_general x1, matrix products, expert_outputs(): jnp.einsum('nesf,efd->nesd', hidden, w_down, preferred_element_type=jnp.f...  6.06 us
    all_to_all x1, starting transfers between devices, body(): lax.all_to_all(expert_outputs(lax.all_to_all(buffer, 'ep', split_axis=0,...  5.17 us
    gather x1, local copies, waits for them, and re-layouts, body(): returned[targets.reshape(-1)].reshape(tok_count, top_count, model_width)  4.22 us
    dot_general x1, matrix products, body(): jnp.dot(shared_hidden, shared_down, preferred_element_type=jnp.float32)  3.87 us
    unnamed x14, local copies, waits for them, and re-layouts  2.91 us
    dot_general x1, matrix products, body(): jnp.dot(normed, shared_gate, preferred_element_type=jnp.float32)  2.74 us
  transfers between devices with their start and end apart: 1, of which 1 were waited for; matrix products, arithmetic and copies ran while one was open for 3% of the time, Pallas kernels for 0%

commit v1 on v0

v1 whole, which is shorter than its diff:
```python
import functools

import jax
import jax.numpy as jnp
from jax import lax
from jax.experimental import pallas as pl
from jax.experimental.pallas import tpu as pltpu
from jax.sharding import PartitionSpec as P

epsilon = 1e-06
MESH = pl.DeviceIdType.MESH
F32, BF16 = jnp.float32, jnp.bfloat16


def flipped(value, mask):
    bit = 1
    while bit <= mask:
        if mask & bit:
            value = value + bit * (1 - 2 * ((value // bit) % 2))
        bit *= 2
    return value


def silu(v):
    return v / (1.0 + jnp.exp(-v))


def dot(a, b):
    return jnp.dot(a, b, preferred_element_type=F32)


def kernel(
    zs, ys, tok_ref, gain_ref, routing_ref, gates_ref, wg_hbm, wu_hbm, wd_hbm, sg_hbm, su_hbm, sd_hbm,
    out_ref, buf, part, from_core, to_y, from_y, to_z, from_z, wg, wu, wd, sg, su, sd,
    w_sem, agz_s, agz_r, agy_s, agy_r, agc_s, agc_r, rsc_s, rsc_r, rsy_s, rsy_r, rsz_s, rsz_r,
):
    toks, width = tok_ref.shape
    top = routing_ref.shape[1]
    lanes = buf.shape[-1] - width
    n = zs * ys * 2
    me = lax.axis_index("ep")
    c = me % 2
    y = (me // 2) % ys
    z = me // (2 * ys)
    oc, oy = 1 - c, (y + 1) % ys

    def dev(zi, yi, ci):
        return {"ep": (zi * ys + yi) * 2 + ci}

    pairs = ((sg_hbm, sg), (su_hbm, su), (sd_hbm, sd), (wg_hbm, wg), (wu_hbm, wu), (wd_hbm, wd))
    loads = [pltpu.make_async_copy(a, b, w_sem.at[i]) for i, (a, b) in enumerate(pairs)]
    for load in loads:
        load.start()

    barrier = pltpu.get_barrier_semaphore()
    peers = [dev(flipped(z, k), y, c) for k in range(1, zs)] + [dev(z, oy, c), dev(z, y, oc)]
    for peer in peers:
        pl.semaphore_signal(barrier, inc=1, device_id=peer, device_id_type=MESH)

    floats = tok_ref[...].astype(F32)
    scale_inv = lax.rsqrt(jnp.mean(floats * floats, axis=-1, keepdims=True) + epsilon)
    normed = (floats * scale_inv * gain_ref[...]).astype(BF16)
    lane = lax.broadcasted_iota(jnp.int32, (toks, lanes), 1)
    weight = jnp.zeros((toks, lanes), F32)
    for k in range(top):
        named = (routing_ref[:, k : k + 1] == lane) | (routing_ref[:, k : k + 1] + n == lane)
        weight = weight + jnp.where(named, gates_ref[:, k : k + 1], 0.0)
    high = weight.astype(BF16).astype(F32)
    low = weight - high
    buf[z, c, y, :, :width] = normed
    buf[z, c, y, :, width:] = jnp.where(lane < n, high, low).astype(BF16)

    pl.semaphore_wait(barrier, len(peers))

    sent = []

    def send(src, dst, s_sem, r_sem, target):
        copy = pltpu.make_async_remote_copy(
            src_ref=src, dst_ref=dst, send_sem=s_sem, recv_sem=r_sem,
            device_id=target, device_id_type=MESH,
        )
        copy.start()
        sent.append(copy)

    def arrived(dst, s_sem, r_sem, source):
        pltpu.make_async_remote_copy(
            src_ref=dst, dst_ref=dst, send_sem=s_sem, recv_sem=r_sem,
            device_id=source, device_id_type=MESH,
        ).wait_recv()

    def forward_y(k):
        block = buf.at[flipped(z, k), c, y]
        send(block, block, agy_s.at[k], agy_r.at[k], dev(z, oy, c))

    def forward_core(k, yi, j):
        block = buf.at[flipped(z, k), c, yi]
        send(block, block, agc_s.at[k, j], agc_r.at[k, j], dev(z, y, oc))

    def take_z(k):
        arrived(buf.at[flipped(z, k), c, y], agz_s.at[k], agz_r.at[k], dev(flipped(z, k), y, c))
        forward_y(k)
        forward_core(k, y, 0)

    def take_y(k):
        arrived(buf.at[flipped(z, k), c, oy], agy_s.at[k], agy_r.at[k], dev(z, oy, c))
        forward_core(k, oy, 1)

    def experts(k):
        zi = flipped(z, k)
        for j, yi in ((0, y), (1, oy)):
            arrived(buf.at[zi, oc, yi], agc_s.at[k, j], agc_r.at[k, j], dev(z, y, oc))
        rows = 2 * ys * toks
        x = buf[zi, :, :, :, :width].reshape(rows, width)
        tags = buf[zi, :, :, :, width:].reshape(rows, lanes).astype(F32)
        where = lax.broadcasted_iota(jnp.int32, (rows, lanes), 1)
        mine = (where == me) | (where == me + n)
        scale = jnp.sum(jnp.where(mine, tags, 0.0), axis=-1, keepdims=True)
        hidden = (silu(dot(x, wg[0])) * dot(x, wu[0])).astype(BF16)
        outs = dot(hidden, wd[0]).astype(BF16).astype(F32) * scale
        part[zi] = outs.astype(BF16).reshape(2, ys, toks, width)
        send(part.at[zi, oc], from_core.at[k], rsc_s.at[k], rsc_r.at[k], dev(z, y, oc))

    def add_core(k):
        zi = flipped(z, k)
        arrived(from_core.at[k], rsc_s.at[k], rsc_r.at[k], dev(z, y, oc))
        both = part[zi, c, oy].astype(F32) + from_core[k, oy].astype(F32)
        to_y[k] = both.astype(BF16)
        send(to_y.at[k], from_y.at[k], rsy_s.at[k], rsy_r.at[k], dev(z, oy, c))

    def add_y(k):
        zi = flipped(z, k)
        arrived(from_y.at[k], rsy_s.at[k], rsy_r.at[k], dev(z, oy, c))
        total = part[zi, c, y].astype(F32) + from_core[k, y].astype(F32) + from_y[k].astype(F32)
        if k == 0:
            return total
        to_z[k] = total.astype(BF16)
        send(to_z.at[k], from_z.at[k], rsz_s.at[k], rsz_r.at[k], dev(zi, y, c))

    for k in range(1, zs):
        own = buf.at[z, c, y]
        send(own, own, agz_s.at[k], agz_r.at[k], dev(flipped(z, k), y, c))
    forward_y(0)
    forward_core(0, y, 0)

    for load in loads[:3]:
        load.wait()
    x = buf[z, c, y, :, :width]
    shared_hidden = (silu(dot(x, sg[...])) * dot(x, su[...])).astype(BF16)
    total = dot(shared_hidden, sd[...])
    for load in loads[3:]:
        load.wait()

    for i in range(zs):
        if i + 1 < zs:
            take_z(i + 1)
        take_y(i)
        experts(i)
        if i >= 1:
            add_core(i - 1)
        if i >= 2:
            got = add_y(i - 2)
            if i == 2:
                total = total + got
    add_core(zs - 1)
    for i in range(max(zs - 2, 0), zs):
        got = add_y(i)
        if i == 0:
            total = total + got
    for k in range(1, zs):
        arrived(from_z.at[k], rsz_s.at[k], rsz_r.at[k], dev(flipped(z, k), y, c))
        total = total + from_z[k].astype(F32)
    out_ref[...] = total.astype(BF16)
    for copy in sent:
        copy.wait_send()


def body(zs, ys, *args):
    tokens, norm_gain, routing, gates, w_gate, w_up, w_down, shared_gate, shared_up, shared_down = args
    toks, width = tokens.shape
    n = zs * ys * 2
    lanes = -(-2 * n // 128) * 128
    dma = pltpu.SemaphoreType.DMA
    vmem = pl.BlockSpec(memory_space=pltpu.VMEM)
    hbm = pl.BlockSpec(memory_space=pl.ANY)
    return pl.pallas_call(
        functools.partial(kernel, zs, ys),
        out_shape=jax.ShapeDtypeStruct((toks, width), BF16),
        in_specs=[vmem] * 4 + [hbm] * 6,
        out_specs=vmem,
        scratch_shapes=[
            pltpu.VMEM((zs, 2, ys, toks, width + lanes), BF16),
            pltpu.VMEM((zs, 2, ys, toks, width), BF16),
            pltpu.VMEM((zs, ys, toks, width), BF16),
            pltpu.VMEM((zs, toks, width), BF16),
            pltpu.VMEM((zs, toks, width), BF16),
            pltpu.VMEM((zs, toks, width), BF16),
            pltpu.VMEM((zs, toks, width), BF16),
        ]
        + [pltpu.VMEM(w.shape, BF16) for w in args[4:]]
        + [dma((6,))]
        + [dma((zs,))] * 4
        + [dma((zs, 2))] * 2
        + [dma((zs,))] * 6,
        compiler_params=pltpu.CompilerParams(
            collective_id=0, has_side_effects=True, vmem_limit_bytes=60 * 1024 * 1024
        ),
    )(tokens, norm_gain.reshape(1, width), *args[2:])


def solution(mesh):
    chips = mesh.shape["ep"] // 2
    ys = 2
    zs = chips // ys
    placed = (
        P(("grp", "ep"), None),
        P(),
        P(("grp", "ep"), None),
        P(("grp", "ep"), None),
        P("ep", None, None),
        P("ep", None, None),
        P("ep", None, None),
        P(),
        P(),
        P(),
    )
    return jax.shard_map(
        functools.partial(body, zs, ys),
        mesh=mesh,
        in_specs=placed,
        out_specs=P(("grp", "ep"), None),
        check_vma=False,
    )
```

time: 130 us -> 49.3 us (0.38)
  the two profiles are of different devices: /device:TPU:15 before, /device:TPU:0 now
where the time goes in v1:
time: 49.3 us; the launch traced here: 49 us
  Pallas kernels  44.7 us (91%)
  local copies, waits for them, and re-layouts  4.29 us (9%)
    pallas_call x1, Pallas kernels, body(): pl.pallas_call(functools.partial(kernel, zs, ys), out_shape=jax.ShapeDtyp...  44.7 us
    unnamed x3, local copies, waits for them, and re-layouts  4.29 us

profile of v1, /device:TPU:0, one launch (start us, length us, event | category | flops | bytes accessed | tf_op | source)
XLA Modules:
  0.0 49.0 jit_solution(11942391633395769461)
XLA Ops:
  0.0 1.4 %copy.11.routing_ref = s32[32,8]{1,0:T(8,128)} copy(s32[32,8]{0,1:T(8,128)} %param.12) | data formatting | bytes 2048 | tf_op args[2]
  1.4 1.4 %copy.12.gates_ref = f32[32,8]{1,0:T(8,128)} copy(f32[32,8]{0,1:T(8,128)} %param.13) | data formatting | bytes 2048 | tf_op args[3]
  2.7 44.7 %shard_map.100 = bf16[32,2048]{1,0:T(8,128)(2,1)} custom-call(bf16[32,2048]{1,0:T(8,128)(2,1)} %tok_ref.1, f32[1,2048]{1,0:T(1,128)} %bitcast.1, s32[32,8]{1,0:T(8,128)} %copy.11.routing_ref, f32[32,8]{1,0:T(8,128)} %copy.12.gates_ref, bf16[1,2048,512]{2,1,0:T(8,128)(2,1)} %wg_hbm.1, bf16[1,2048,512]{2,1,0:T(8,128)(2,1)} %wu_hbm.1, ...), custom_call_target="tpu_custom_call" | custom-call | tf_op jit(solution)/shard_map/pallas_call | solution.py:185
  47.5 1.6 %copy.14 = bf16[32,2048]{1,0:T(8,128)(2,1)} copy(bf16[32,2048]{1,0:T(8,128)(2,1)} %shard_map.100) | data formatting | bytes 262144

commit v2 on v1

v2 whole, which is shorter than its diff:
```python
import functools

import jax
import jax.numpy as jnp
from jax import lax
from jax.experimental import pallas as pl
from jax.experimental.pallas import tpu as pltpu
from jax.sharding import PartitionSpec as P

epsilon = 1e-06
MESH = pl.DeviceIdType.MESH
F32, BF16 = jnp.float32, jnp.bfloat16


def flipped(value, mask):
    bit = 1
    while bit <= mask:
        if mask & bit:
            value = value + bit * (1 - 2 * ((value // bit) % 2))
        bit *= 2
    return value


def silu(v):
    return v / (1.0 + jnp.exp(-v))


def dot(a, b):
    return jnp.dot(a, b, preferred_element_type=F32)


def kernel(
    zs, ys, tok_ref, gain_ref, routing_ref, gates_ref, wg_hbm, wu_hbm, wd_hbm, sg_hbm, su_hbm, sd_hbm,
    out_ref, buf, part, from_core, to_y, from_y, to_z, from_z, sums, wg, wu, wd, sg, su, sd,
    w_sem, agz_s, agz_r, agy_s, agy_r, agc_s, agc_r, rsc_s, rsc_r, rsy_s, rsy_r, rsz_s, rsz_r,
):
    toks, width = tok_ref.shape
    top = routing_ref.shape[0]
    lanes = buf.shape[-1] - width
    n = zs * ys * 2
    me = lax.axis_index("ep")
    c = me % 2
    y = (me // 2) % ys
    z = me // (2 * ys)
    oc, oy = 1 - c, (y + 1) % ys

    def dev(zi, yi, ci):
        return {"ep": (zi * ys + yi) * 2 + ci}

    pairs = ((sg_hbm, sg), (su_hbm, su), (sd_hbm, sd), (wg_hbm, wg), (wu_hbm, wu), (wd_hbm, wd))
    loads = [pltpu.make_async_copy(a, b, w_sem.at[i]) for i, (a, b) in enumerate(pairs)]
    for load in loads:
        load.start()

    barrier = pltpu.get_barrier_semaphore()
    peers = [dev(flipped(z, k), y, c) for k in range(1, zs)] + [dev(z, oy, c), dev(z, y, oc)]
    for peer in peers:
        pl.semaphore_signal(barrier, inc=1, device_id=peer, device_id_type=MESH)

    floats = tok_ref[...].astype(F32)
    scale_inv = lax.rsqrt(jnp.mean(floats * floats, axis=-1, keepdims=True) + epsilon)
    normed = (floats * scale_inv * gain_ref[...]).astype(BF16)
    lane = lax.broadcasted_iota(jnp.int32, (toks, lanes), 1)
    tag = lax.broadcasted_iota(jnp.int32, (lanes, toks), 0)
    weight = jnp.zeros((lanes, toks), F32)
    for k in range(top):
        named = (routing_ref[k : k + 1, :] == tag) | (routing_ref[k : k + 1, :] + n == tag)
        weight = weight + jnp.where(named, gates_ref[k : k + 1, :], 0.0)
    weight = weight.T
    high = weight.astype(BF16).astype(F32)
    low = weight - high
    buf[z, c, y, :, :width] = normed
    buf[z, c, y, :, width:] = jnp.where(lane < n, high, low).astype(BF16)

    pl.semaphore_wait(barrier, len(peers))

    parts = 2 if toks % 32 == 0 else 1
    size = toks // parts
    gather_order = list(range(1, zs))
    sent = []

    def send(src, dst, s_sem, r_sem, target):
        copy = pltpu.make_async_remote_copy(
            src_ref=src, dst_ref=dst, send_sem=s_sem, recv_sem=r_sem,
            device_id=target, device_id_type=MESH,
        )
        copy.start()
        sent.append(copy)

    def piece(zi, ci, yi, h):
        return buf.at[zi, ci, yi, pl.ds(h * size, size)]

    def arrived(dst, s_sem, r_sem, source):
        pltpu.make_async_remote_copy(
            src_ref=dst, dst_ref=dst, send_sem=s_sem, recv_sem=r_sem,
            device_id=source, device_id_type=MESH,
        ).wait_recv()

    def forward_y(k, h):
        block = piece(flipped(z, k), c, y, h)
        send(block, block, agy_s.at[k, h], agy_r.at[k, h], dev(z, oy, c))

    def forward_core(k, yi, j, h):
        block = piece(flipped(z, k), c, yi, h)
        send(block, block, agc_s.at[k, j, h], agc_r.at[k, j, h], dev(z, y, oc))

    def take_z(k):
        for h in range(parts):
            arrived(piece(flipped(z, k), c, y, h), agz_s.at[k, h], agz_r.at[k, h], dev(flipped(z, k), y, c))
            forward_y(k, h)
            forward_core(k, y, 0, h)

    def take_y(k):
        for h in range(parts):
            arrived(piece(flipped(z, k), c, oy, h), agy_s.at[k, h], agy_r.at[k, h], dev(z, oy, c))
            forward_core(k, oy, 1, h)

    def experts(k):
        zi = flipped(z, k)
        for j, yi in ((0, y), (1, oy)):
            for h in range(parts):
                arrived(piece(zi, oc, yi, h), agc_s.at[k, j, h], agc_r.at[k, j, h], dev(z, y, oc))
        rows = 2 * ys * toks
        x = buf[zi, :, :, :, :width].reshape(rows, width)
        tags = buf[zi, :, :, :, width:].reshape(rows, lanes).astype(F32)
        where = lax.broadcasted_iota(jnp.int32, (rows, lanes), 1)
        mine = (where == me) | (where == me + n)
        scale = jnp.sum(jnp.where(mine, tags, 0.0), axis=-1, keepdims=True)
        hidden = (silu(dot(x, wg[0])) * dot(x, wu[0])).astype(BF16)
        outs = dot(hidden, wd[0]).astype(BF16).astype(F32) * scale
        part[zi] = outs.astype(BF16).reshape(2, ys, toks, width)
        for j, yi in ((0, oy), (1, y)):
            send(part.at[zi, oc, yi], from_core.at[k, yi], rsc_s.at[k, j], rsc_r.at[k, j], dev(z, y, oc))

    def add_core(k):
        zi = flipped(z, k)
        arrived(from_core.at[k, oy], rsc_s.at[k, 0], rsc_r.at[k, 0], dev(z, y, oc))
        for h in range(parts):
            at = pl.ds(h * size, size)
            both = part[zi, c, oy, at].astype(F32) + from_core[k, oy, at].astype(F32)
            to_y[k, at] = both.astype(BF16)
            send(to_y.at[k, at], from_y.at[k, at], rsy_s.at[k, h], rsy_r.at[k, h], dev(z, oy, c))

    def add_y(k):
        zi = flipped(z, k)
        arrived(from_core.at[k, y], rsc_s.at[k, 1], rsc_r.at[k, 1], dev(z, y, oc))
        for h in range(parts):
            at = pl.ds(h * size, size)
            arrived(from_y.at[k, at], rsy_s.at[k, h], rsy_r.at[k, h], dev(z, oy, c))
            total = part[zi, c, y, at].astype(F32) + from_core[k, y, at].astype(F32) + from_y[k, at].astype(F32)
            if k == 0:
                sums[at] = sums[at] + total
            else:
                to_z[k, at] = total.astype(BF16)
                send(to_z.at[k, at], from_z.at[k, at], rsz_s.at[k, h], rsz_r.at[k, h], dev(zi, y, c))

    for h in range(parts):
        forward_y(0, h)
        forward_core(0, y, 0, h)
    for k in gather_order:
        for h in range(parts):
            own = piece(z, c, y, h)
            send(own, own, agz_s.at[k, h], agz_r.at[k, h], dev(flipped(z, k), y, c))

    for load in loads[:3]:
        load.wait()
    x = buf[z, c, y, :, :width]
    shared_hidden = (silu(dot(x, sg[...])) * dot(x, su[...])).astype(BF16)
    sums[...] = dot(shared_hidden, sd[...])
    for load in loads[3:]:
        load.wait()

    def program():
        for i in range(zs):
            if i + 1 < zs:
                yield take_z, i + 1
            yield take_y, i
            yield experts, i
            if i == zs - 2:
                for k in range(zs - 2, 0, -1):
                    yield add_core, k
        yield add_core, zs - 1
        yield add_core, 0
        for k in range(zs - 2, 0, -1):
            yield add_y, k
        yield add_y, zs - 1
        yield add_y, 0

    for step, k in program():
        step(k)
    total = sums[...]
    for k in gather_order:
        for h in range(parts):
            at = pl.ds(h * size, size)
            arrived(from_z.at[k, at], rsz_s.at[k, h], rsz_r.at[k, h], dev(flipped(z, k), y, c))
        total = total + from_z[k].astype(F32)
    out_ref[...] = total.astype(BF16)
    for copy in sent:
        copy.wait_send()


def body(zs, ys, *args):
    tokens, norm_gain, routing, gates, w_gate, w_up, w_down, shared_gate, shared_up, shared_down = args
    toks, width = tokens.shape
    n = zs * ys * 2
    lanes = -(-2 * n // 128) * 128
    dma = pltpu.SemaphoreType.DMA
    vmem = pl.BlockSpec(memory_space=pltpu.VMEM)
    hbm = pl.BlockSpec(memory_space=pl.ANY)
    return pl.pallas_call(
        functools.partial(kernel, zs, ys),
        out_shape=pltpu.VMEM((toks, width), BF16),
        in_specs=[vmem] * 4 + [hbm] * 6,
        out_specs=vmem,
        scratch_shapes=[
            pltpu.VMEM((zs, 2, ys, toks, width + lanes), BF16),
            pltpu.VMEM((zs, 2, ys, toks, width), BF16),
            pltpu.VMEM((zs, ys, toks, width), BF16),
            pltpu.VMEM((zs, toks, width), BF16),
            pltpu.VMEM((zs, toks, width), BF16),
            pltpu.VMEM((zs, toks, width), BF16),
            pltpu.VMEM((zs, toks, width), BF16),
            pltpu.VMEM((toks, width), F32),
        ]
        + [pltpu.VMEM(w.shape, BF16) for w in args[4:]]
        + [dma((6,))]
        + [dma((zs, 2))] * 4
        + [dma((zs, 2, 2))] * 2
        + [dma((zs, 2))] * 6,
        compiler_params=pltpu.CompilerParams(
            collective_id=0, has_side_effects=True, vmem_limit_bytes=60 * 1024 * 1024
        ),
    )(tokens, norm_gain.reshape(1, width), routing.T, gates.T, *args[4:])


def solution(mesh):
    chips = mesh.shape["ep"] // 2
    ys = 2
    zs = chips // ys
    placed = (
        P(("grp", "ep"), None),
        P(),
        P(("grp", "ep"), None),
        P(("grp", "ep"), None),
        P("ep", None, None),
        P("ep", None, None),
        P("ep", None, None),
        P(),
        P(),
        P(),
    )
    return jax.shard_map(
        functools.partial(body, zs, ys),
        mesh=mesh,
        in_specs=placed,
        out_specs=P(("grp", "ep"), None),
        check_vma=False,
    )
```

time: 49.3 us -> 41.3 us (0.84)
  Pallas kernels: 44.7 us -> 40.5 us
  local copies, waits for them, and re-layouts: 4.29 us -> 0.66 us
    pallas_call x1, Pallas kernels: 44.7 us -> 40.5 us  [body(): pl.pallas_call(functools.partial(kernel, zs, ys), out_shape=pltpu.VMEM((t...]
    unnamed x3 -> x1, local copies, waits for them, and re-layouts: 4.29 us -> 0.66 us
where the time goes in v2:
time: 41.3 us; the launch traced here: 41.2 us
  Pallas kernels  40.5 us (98%)
  local copies, waits for them, and re-layouts  0.66 us (2%)
    pallas_call x1, Pallas kernels, body(): pl.pallas_call(functools.partial(kernel, zs, ys), out_shape=pltpu.VMEM((t...  40.5 us

profile of v2, /device:TPU:0, one launch (start us, length us, event | category | flops | bytes accessed | tf_op | source)
XLA Modules:
  0.0 41.2 jit_solution(16904115250416715844)
XLA Ops:
  0.0 40.5 %shard_map.100 = bf16[32,2048]{1,0:T(8,128)(2,1)S(1)} custom-call(bf16[32,2048]{1,0:T(8,128)(2,1)} %tok_ref.1, f32[1,2048]{1,0:T(1,128)} %bitcast.3, s32[8,32]{1,0:T(8,128)} %bitcast.4, f32[8,32]{1,0:T(8,128)} %bitcast.5, bf16[1,2048,512]{2,1,0:T(8,128)(2,1)} %wg_hbm.1, bf16[1,2048,512]{2,1,0:T(8,128)(2,1)} %wu_hbm.1, bf16[1,512,2048]{2,1,0:T(8,128)(2,1)} %wd_hbm.1, ...), custom_call_target="tpu_custom_call" | custom-call | tf_op jit(solution)/shard_map/pallas_call | solution.py:210
  40.5 0.7 %copy.12 = bf16[32,2048]{1,0:T(8,128)(2,1)} copy(bf16[32,2048]{1,0:T(8,128)(2,1)S(1)} %shard_map.100) | data formatting | bytes 262144

commit v3 on v2

--- a/solution.py
+++ b/solution.py
@@ -53,6 +53,7 @@
         load.start()
 
     barrier = pltpu.get_barrier_semaphore()
+    gather_order = [1] + list(range(2, zs, 2))
     peers = [dev(flipped(z, k), y, c) for k in range(1, zs)] + [dev(z, oy, c), dev(z, y, oc)]
     for peer in peers:
         pl.semaphore_signal(barrier, inc=1, device_id=peer, device_id_type=MESH)
@@ -76,7 +77,6 @@
 
     parts = 2 if toks % 32 == 0 else 1
     size = toks // parts
-    gather_order = list(range(1, zs))
     sent = []
 
     def send(src, dst, s_sem, r_sem, target):
@@ -106,7 +106,10 @@
 
     def take_z(k):
         for h in range(parts):
-            arrived(piece(flipped(z, k), c, y, h), agz_s.at[k, h], agz_r.at[k, h], dev(flipped(z, k), y, c))
+            block = piece(flipped(z, k), c, y, h)
+            arrived(block, agz_s.at[k, h], agz_r.at[k, h], dev(flipped(z, 1 if k % 2 else k), y, c))
+            if k % 2 == 0:
+                send(block, block, agz_s.at[k + 1, h], agz_r.at[k + 1, h], dev(flipped(z, 1), y, c))
             forward_y(k, h)
             forward_core(k, y, 0, h)
 
@@ -151,8 +154,12 @@
             if k == 0:
                 sums[at] = sums[at] + total
             else:
+                if k % 2 and k > 1:
+                    arrived(from_z.at[k - 1, at], rsz_s.at[k - 1, h], rsz_r.at[k - 1, h], dev(flipped(z, 1), y, c))
+                    total = total + from_z[k - 1, at].astype(F32)
                 to_z[k, at] = total.astype(BF16)
-                send(to_z.at[k, at], from_z.at[k, at], rsz_s.at[k, h], rsz_r.at[k, h], dev(zi, y, c))
+                target = dev(flipped(z, k if k % 2 else 1), y, c)
+                send(to_z.at[k, at], from_z.at[k, at], rsz_s.at[k, h], rsz_r.at[k, h], target)
 
     for h in range(parts):
         forward_y(0, h)
@@ -171,25 +178,28 @@
         load.wait()
 
     def program():
+        for k in range(1, min(zs, 3)):
+            yield take_z, k
+        for k in range(min(zs, 2)):
+            yield take_y, k
         for i in range(zs):
-            if i + 1 < zs:
-                yield take_z, i + 1
-            yield take_y, i
+            if i >= 2:
+                yield add_core, i - 1
             yield experts, i
-            if i == zs - 2:
-                for k in range(zs - 2, 0, -1):
-                    yield add_core, k
-        yield add_core, zs - 1
+            if i + 3 < zs:
+                yield take_z, i + 3
+            if 1 <= i < zs - 1:
+                yield take_y, i + 1
+        if zs > 1:
+            yield add_core, zs - 1
         yield add_core, 0
-        for k in range(zs - 2, 0, -1):
+        for k in list(range(2, zs, 2)) + list(range(1, zs, 2)) + [0]:
             yield add_y, k
-        yield add_y, zs - 1
-        yield add_y, 0
 
     for step, k in program():
         step(k)
     total = sums[...]
-    for k in gather_order:
+    for k in range(1, zs, 2):
         for h in range(parts):
             at = pl.ds(h * size, size)
             arrived(from_z.at[k, at], rsz_s.at[k, h], rsz_r.at[k, h], dev(flipped(z, k), y, c))

time: 41.3 us -> 40.4 us (0.978)
  Pallas kernels: 40.5 us -> 39.6 us
    pallas_call x1, Pallas kernels: 40.5 us -> 39.6 us  [body(): pl.pallas_call(functools.partial(kernel, zs, ys), out_shape=pltpu.VMEM((t...]
where the time goes in v3:
time: 40.4 us; the launch traced here: 40.3 us
  Pallas kernels  39.6 us (98%)
  local copies, waits for them, and re-layouts  0.66 us (2%)
    pallas_call x1, Pallas kernels, body(): pl.pallas_call(functools.partial(kernel, zs, ys), out_shape=pltpu.VMEM((t...  39.6 us

profile of v3, /device:TPU:0, one launch (start us, length us, event | category | flops | bytes accessed | tf_op | source)
XLA Modules:
  0.0 40.3 jit_solution(13546118397769686802)
XLA Ops:
  0.0 39.6 %shard_map.100 = bf16[32,2048]{1,0:T(8,128)(2,1)S(1)} custom-call(bf16[32,2048]{1,0:T(8,128)(2,1)} %tok_ref.1, f32[1,2048]{1,0:T(1,128)} %bitcast.3, s32[8,32]{1,0:T(8,128)} %bitcast.4, f32[8,32]{1,0:T(8,128)} %bitcast.5, bf16[1,2048,512]{2,1,0:T(8,128)(2,1)} %wg_hbm.1, bf16[1,2048,512]{2,1,0:T(8,128)(2,1)} %wu_hbm.1, bf16[1,512,2048]{2,1,0:T(8,128)(2,1)} %wd_hbm.1, ...), custom_call_target="tpu_custom_call" | custom-call | tf_op jit(solution)/shard_map/pallas_call | solution.py:220
  39.6 0.7 %copy.12 = bf16[32,2048]{1,0:T(8,128)(2,1)} copy(bf16[32,2048]{1,0:T(8,128)(2,1)S(1)} %shard_map.100) | data formatting | bytes 262144

commit v4 on v3

--- a/solution.py
+++ b/solution.py
@@ -169,17 +169,19 @@
             own = piece(z, c, y, h)
             send(own, own, agz_s.at[k, h], agz_r.at[k, h], dev(flipped(z, k), y, c))
 
-    for load in loads[:3]:
-        load.wait()
-    x = buf[z, c, y, :, :width]
-    shared_hidden = (silu(dot(x, sg[...])) * dot(x, su[...])).astype(BF16)
-    sums[...] = dot(shared_hidden, sd[...])
-    for load in loads[3:]:
-        load.wait()
+    def shared(_):
+        for load in loads[:3]:
+            load.wait()
+        x = buf[z, c, y, :, :width]
+        shared_hidden = (silu(dot(x, sg[...])) * dot(x, su[...])).astype(BF16)
+        sums[...] = dot(shared_hidden, sd[...])
+        for load in loads[3:]:
+            load.wait()
 
     def program():
         for k in range(1, min(zs, 3)):
             yield take_z, k
+        yield shared, 0
         for k in range(min(zs, 2)):
             yield take_y, k
         for i in range(zs):

time: 40.4 us -> 40.4 us (level)
  no operation moved by 1% of the time
where the time goes in v4:
time: 40.4 us; the launch traced here: 40.3 us
  Pallas kernels  39.6 us (98%)
  local copies, waits for them, and re-layouts  0.66 us (2%)
    pallas_call x1, Pallas kernels, body(): pl.pallas_call(functools.partial(kernel, zs, ys), out_shape=pltpu.VMEM((t...  39.6 us

profile of v4, /device:TPU:0, one launch (start us, length us, event | category | flops | bytes accessed | tf_op | source)
XLA Modules:
  0.0 40.3 jit_solution(9231046210754073267)
XLA Ops:
  0.0 39.6 %shard_map.100 = bf16[32,2048]{1,0:T(8,128)(2,1)S(1)} custom-call(bf16[32,2048]{1,0:T(8,128)(2,1)} %tok_ref.1, f32[1,2048]{1,0:T(1,128)} %bitcast.3, s32[8,32]{1,0:T(8,128)} %bitcast.4, f32[8,32]{1,0:T(8,128)} %bitcast.5, bf16[1,2048,512]{2,1,0:T(8,128)(2,1)} %wg_hbm.1, bf16[1,2048,512]{2,1,0:T(8,128)(2,1)} %wu_hbm.1, bf16[1,512,2048]{2,1,0:T(8,128)(2,1)} %wd_hbm.1, ...), custom_call_target="tpu_custom_call" | custom-call | tf_op jit(solution)/shard_map/pallas_call | solution.py:222
  39.6 0.7 %copy.12 = bf16[32,2048]{1,0:T(8,128)(2,1)} copy(bf16[32,2048]{1,0:T(8,128)(2,1)S(1)} %shard_map.100) | data formatting | bytes 262144
